TPU v7x, 32 devices: a whole 2x2x4 slice. The times are simulated.
32 devices in a mesh: sp: 8 (over z, y), tp: 4 (over x, core).
Axes of the slice: x: 2, y: 2, z: 4, core: 2. Of those that a mesh axis runs over, the one named last changes fastest.
Arguments:
- queries: bfloat16 [6144, 1536], P('sp', 'tp'), may hold values from -130 to 130, as said below
- keys: bfloat16 [6144, 512], P('sp', 'tp'), may hold values from -6 to 6
- values: bfloat16 [6144, 512], P('sp', 'tp'), may hold values from -6 to 6
- residual: bfloat16 [6144, 2048], P(('sp', 'tp')), may hold values from -6 to 6
- sinks: float32 [12], P('tp'), may hold values from 2 to 6
- out_weight: bfloat16 [1536, 2048], P('tp'), may hold values from -0.15625 to 0.15625
- up_weight: bfloat16 [2048, 8192], P('sp', 'tp'), may hold values from -0.125 to 0.125
- down_weight: bfloat16 [8192, 2048], P('tp', 'sp'), may hold values from -0.0625 to 0.0625
- gains: float32 [2, 2048], replicated, may hold values from 0.1 to 1.9
- biases: float32 [2, 2048], replicated, may hold values from -3 to 3
Outputs:
- layer_out: bfloat16 [6144, 2048], P(('sp', 'tp'))
Inputs may be any that keep to these rules, and one draw needn't show every extreme that they name: `queries`: entries of order one, with some rows far larger in some draws.
All inputs are finite; a program needn't handle non-finite values.
Results may differ from a plain program's by a relative error of at most 0.0095.
Values may be sent and summed in bfloat16 or wider, within the bound.
A program may use at most 128 MiB of HBM per device.

v0:
```python
import jax
import jax.numpy as jnp
from jax import lax
from jax.sharding import PartitionSpec as P

HEADS = 12
HEAD = 128
WINDOW = 128


deep_alpha = 1.6817928
norm_eps = 1e-05
neg_big = -1e30


def from_behind(block, axis, distance):
    devices = range(lax.axis_size(axis))
    route = [(i - distance, i) for i in devices if i - distance in devices]
    return lax.ppermute(block, axis, route)


def layer_norm(stream, gain, bias):
    mean = jnp.mean(stream, axis=-1, keepdims=True)
    spread = jnp.mean(jnp.square(stream - mean), axis=-1, keepdims=True)
    return ((stream - mean) * lax.rsqrt(spread + norm_eps) * gain + bias).astype(jnp.bfloat16)


def attend(queries, keys, values, before, sinks, offset, rank_tp):
    tokens = keys.shape[0]
    kv_local = keys.shape[1] // HEAD
    heads_local = sinks.shape[0]
    group = heads_local // kv_local
    blocks = tokens // WINDOW
    q_blocks = queries.reshape(blocks, WINDOW, kv_local, group, HEAD)
    key_ext = jnp.concatenate([before[0], keys], axis=0).reshape(tokens + WINDOW, kv_local, HEAD)
    val_ext = jnp.concatenate([before[1], values], axis=0).reshape(tokens + WINDOW, kv_local, HEAD)
    key_win = jnp.concatenate(
        [
            key_ext[:tokens].reshape(blocks, WINDOW, kv_local, HEAD),
            key_ext[WINDOW:].reshape(blocks, WINDOW, kv_local, HEAD),
        ],
        axis=1,
    )
    val_win = jnp.concatenate(
        [
            val_ext[:tokens].reshape(blocks, WINDOW, kv_local, HEAD),
            val_ext[WINDOW:].reshape(blocks, WINDOW, kv_local, HEAD),
        ],
        axis=1,
    )
    logits = jnp.einsum(
        "nqkgd,nskd->nkgqs", q_blocks, key_win, preferred_element_type=jnp.float32
    ) * HEAD ** (-0.5)
    q_index = jnp.arange(WINDOW, dtype=jnp.int32)[:, None]
    k_index = jnp.arange(2 * WINDOW, dtype=jnp.int32)[None, :]
    dist = q_index + WINDOW - k_index
    block_id = jnp.arange(blocks, dtype=jnp.int32)[:, None, None]
    key_pos = offset + block_id * WINDOW - WINDOW + k_index
    valid = (dist >= 0) & (dist < WINDOW) & (key_pos >= 0)
    heads = (jnp.arange(heads_local, dtype=jnp.int32) + rank_tp * heads_local).astype(jnp.float32)
    slopes = jnp.exp2(-8.0 * (heads + 1.0) / HEADS).reshape(kv_local, group)[:, :, None, None]
    logits = logits - slopes * dist.astype(jnp.float32)
    logits = jnp.where(valid[:, None, None], logits, neg_big)
    sink = sinks.reshape(kv_local, group)[:, :, None, None]
    top = jnp.maximum(jnp.max(logits, axis=-1, keepdims=True), sink)
    probs = jnp.exp(logits - top)
    denom = jnp.sum(probs, axis=-1, keepdims=True) + jnp.exp(sink - top)
    weight = (probs / denom).astype(jnp.bfloat16)
    attended = jnp.einsum("nkgqs,nskd->nqkgd", weight, val_win, preferred_element_type=jnp.float32)
    return attended.astype(jnp.bfloat16).reshape(tokens, heads_local * HEAD)


def on_device(
    queries, keys, values, residual, sinks, out_weight, up_weight, down_weight, gains, biases
):
    tokens = queries.shape[0]
    rank_tp = lax.axis_index("tp")
    up_full, down_full = (
        lax.all_gather(up_weight, "sp", axis=0, tiled=True),
        lax.all_gather(down_weight, "sp", axis=1, tiled=True),
    )
    tails = jnp.stack([keys[tokens - WINDOW :], values[tokens - WINDOW :]])
    before = from_behind(tails, "sp", 1)
    offset = lax.axis_index("sp") * tokens
    attended = attend(queries, keys, values, before, sinks, offset, rank_tp)
    mix = lax.psum_scatter(
        jnp.dot(attended, out_weight, preferred_element_type=jnp.float32).astype(jnp.bfloat16),
        "tp",
        scatter_dimension=0,
        tiled=True,
    ).astype(jnp.float32)
    normed = layer_norm(deep_alpha * residual.astype(jnp.float32) + mix, gains[0], biases[0])
    whole = lax.all_gather(normed, "tp", axis=0, tiled=True)
    upward = jnp.dot(whole, up_full, preferred_element_type=jnp.float32)
    act = jnp.square(jax.nn.relu(upward)).astype(jnp.bfloat16)
    terms = jnp.dot(act, down_full, preferred_element_type=jnp.float32)
    ffn = lax.psum_scatter(
        terms.astype(jnp.bfloat16), "tp", scatter_dimension=0, tiled=True
    ).astype(jnp.float32)
    return layer_norm(deep_alpha * normed.astype(jnp.float32) + ffn, gains[1], biases[1])


def solution(mesh):
    return jax.shard_map(
        on_device,
        mesh=mesh,
        in_specs=(
            P("sp", "tp"),
            P("sp", "tp"),
            P("sp", "tp"),
            P(("sp", "tp"), None),
            P("tp"),
            P("tp", None),
            P("sp", "tp"),
            P("tp", "sp"),
            P(),
            P(),
        ),
        out_specs=P(("sp", "tp"), None),
        check_vma=False,
    )
```

profile of v0, /device:TPU:0, one launch (start us, length us, event | category | flops | bytes accessed | tf_op | source)
XLA Modules:
  0.0 408.7 jit_solution(9440139312392734191)
XLA Ops:
  6.5 0.9 slice_bitcast_fusion.2
  7.5 0.6 pad_maximum_fusion.2
  8.1 5.5 %collective-permute-start = (bf16[2,128,128]{2,1,0:T(8,128)(2,1)}, bf16[2,128,128]{2,1,0:T(8,128)(2,1)}, u32[]{:S(2)}, u32[]{:S(2)}) collective-permute-start(bf16[2,128,128]{2,1,0:T(8,128)(2,1)} %pad_maximum_fusion.2), channel_id=1, source_target_pairs={{0,4},{4,8},{8,12},{12,16},{16,20},{20,24},{24,28},{1,5},{5,9},{9,... | collective-permute-start | bytes 196616 | tf_op jit(solution)/shard_map/ppermute | solution.py:19
  13.9 1.0 broadcast_and_fusion
  15.3 0.8 slice_bitcast_fusion.1
  16.1 0.9 pad_maximum_fusion
  17.0 1.7 fusion.21
  18.8 1.3 copy-done.5
  20.7 2.2 fusion.2
  23.3 3.5 convolution_convert_fusion.1
  26.9 0.6 copy-done.8
  27.6 39.3 %reduce-scatter.3.cloned.1.call-done = bf16[192,2048]{1,0:T(8,128)(2,1)} async-done(((bf16[768,2048]{1,0:T(8,128)(2,1)}), bf16[192,2048]{1,0:T(8,128)(2,1)}) %reduce-scatter.3.cloned.1.call-update) | async-done | bytes 786448 | tf_op jit(solution)/shard_map/reduce_scatter | solution.py:86
  66.9 1.5 fusion.3
  69.0 1.4 add_convert_fusion.1
  70.4 0.7 all-gather.6.cloned.1.call-update
  71.1 0.5 all-gather.8.cloned.1.call-update
  71.9 27.1 %all-gather.4.cloned.1.call-done = bf16[768,2048]{1,0:T(8,128)(2,1)} async-done(((bf16[192,2048]{1,0:T(8,128)(2,1)}), bf16[768,2048]{1,0:T(8,128)(2,1)}) %all-gather.4.cloned.1.call-update) | async-done | bytes 3145744 | tf_op jit(solution)/shard_map/all_gather | solution.py:93
  99.0 126.6 %all-gather.6.cloned.1.call-done = bf16[2048,2048]{1,0:T(8,128)(2,1)} async-done(((bf16[256,2048]{1,0:T(8,128)(2,1)}), bf16[2048,2048]{1,0:T(8,128)(2,1)}) %all-gather.6.cloned.1.call-update) | async-done | bytes 8388624 | tf_op jit(solution)/shard_map/all_gather | solution.py:79
  225.6 11.9 %multiply_convert_fusion = bf16[768,2048]{1,0:T(8,128)(2,1)} fusion(bf16[768,2048]{1,0:T(8,128)(2,1)} %all-gather.4.cloned.1.call-done, bf16[2048,2048]{1,0:T(8,128)(2,1)} %all-gather.6.cloned.1.call-done), kind=kOutput, calls=%fused_computation | convolution fusion | flops 6447169536 | bytes 14680064 | tf_op jit(solution)/shard_map/dot_general | solution.py:94
  237.5 113.2 %all-gather.8.cloned.1.call-done = bf16[2048,2048]{1,0:T(8,128)(2,1)} async-done(((bf16[2048,256]{1,0:T(8,128)(2,1)}), bf16[2048,2048]{1,0:T(8,128)(2,1)}) %all-gather.8.cloned.1.call-update) | async-done | bytes 8388624 | tf_op jit(solution)/shard_map/all_gather | solution.py:80
  350.7 11.8 %convolution_convert_fusion = bf16[768,2048]{1,0:T(8,128)(2,1)} fusion(bf16[768,2048]{1,0:T(8,128)(2,1)} %multiply_convert_fusion, bf16[2048,2048]{1,0:T(8,128)(2,1)} %all-gather.8.cloned.1.call-done), kind=kOutput, calls=%fused_computation.1 | convolution fusion | flops 6444023808 | bytes 14680064 | tf_op jit(solution)/shard_map/dot_general | solution.py:96
  362.6 36.2 %reduce-scatter.5.cloned.1.call-done = bf16[192,2048]{1,0:T(8,128)(2,1)} async-done(((bf16[768,2048]{1,0:T(8,128)(2,1)}), bf16[192,2048]{1,0:T(8,128)(2,1)}) %reduce-scatter.5.cloned.1.call-update) | async-done | bytes 786448 | tf_op jit(solution)/shard_map/reduce_scatter | solution.py:97
  398.8 1.5 fusion.4
  400.8 1.4 add_convert_fusion
  (52 shorter events, 3.1 us)
Async XLA Ops:
  6.5 16.8 %copy-start = (bf16[384,2048]{1,0:T(8,128)(2,1)S(1)}, bf16[384,2048]{1,0:T(8,128)(2,1)}, u32[]{:S(2)}) copy-start(bf16[384,2048]{1,0:T(8,128)(2,1)} %param.15) | copy-start | bytes 4718596
  6.5 8.5 %copy-start.6 = (bf16[768,128]{1,0:T(8,128)(2,1)S(1)}, bf16[768,128]{1,0:T(8,128)(2,1)}, u32[]{:S(2)}) copy-start(bf16[768,128]{1,0:T(8,128)(2,1)} %param.12) | copy-start | bytes 589828
  6.5 8.3 %copy-start.7 = (bf16[768,384]{1,0:T(8,128)(2,1)S(1)}, bf16[768,384]{1,0:T(8,128)(2,1)}, u32[]{:S(2)}) copy-start(bf16[768,384]{1,0:T(8,128)(2,1)} %param.10) | copy-start | bytes 1769476
  6.5 60.4 %reduce-scatter.3.cloned.1.call-start = ((), (), s32[]{:S(2)}) async-start(), calls=%async_computation.2 | async-start | bytes 3932160 | tf_op jit(solution)/shard_map/reduce_scatter | solution.py:86
  8.1 7.1 %collective-permute-start = (bf16[2,128,128]{2,1,0:T(8,128)(2,1)}, bf16[2,128,128]{2,1,0:T(8,128)(2,1)}, u32[]{:S(2)}, u32[]{:S(2)}) collective-permute-start(bf16[2,128,128]{2,1,0:T(8,128)(2,1)} %pad_maximum_fusion.2), channel_id=1, source_target_pairs={{0,4},{4,8},{8,12},{12,16},{16,20},{20,24},{24,28},{1,5},{5,9},{9,... | collective-permute-start | bytes 196616 | tf_op jit(solution)/shard_map/ppermute | solution.py:19
  17.0 1.7 copy-start.10
  18.7 1.4 copy-start.5
  26.8 0.7 copy-start.8
  26.8 0.7 copy-start.9
  26.8 40.1 %copy-start.2 = (bf16[192,2048]{1,0:T(8,128)(2,1)S(1)}, bf16[192,2048]{1,0:T(8,128)(2,1)}, u32[]{:S(2)}) copy-start(bf16[192,2048]{1,0:T(8,128)(2,1)} %param.13) | copy-start | bytes 2359300
  26.9 72.1 %all-gather.4.cloned.1.call-start = ((), (), s32[]{:S(2)}) async-start(), calls=%async_computation.3 | async-start | bytes 3932160 | tf_op jit(solution)/shard_map/all_gather | solution.py:93
  66.9 1.6 copy-start.3
  70.3 155.3 %all-gather.6.cloned.1.call-start = ((), (), s32[]{:S(2)}) async-start(), calls=%async_computation.4 | async-start | bytes 9437184 | tf_op jit(solution)/shard_map/all_gather | solution.py:79
  71.1 279.6 %all-gather.8.cloned.1.call-start = ((), (), s32[]{:S(2)}) async-start(), calls=%async_computation.5 | async-start | bytes 9437184 | tf_op jit(solution)/shard_map/all_gather | solution.py:80
  71.7 327.1 %reduce-scatter.5.cloned.1.call-start = ((), (), s32[]{:S(2)}) async-start(), calls=%async_computation.6 | async-start | bytes 3932160 | tf_op jit(solution)/shard_map/reduce_scatter | solution.py:97
  362.5 36.2 %copy-start.1 = (bf16[192,2048]{1,0:T(8,128)(2,1)S(1)}, bf16[192,2048]{1,0:T(8,128)(2,1)}, u32[]{:S(2)}) copy-start(bf16[192,2048]{1,0:T(8,128)(2,1)} %add_convert_fusion.1) | copy-start | bytes 2359300
  398.8 1.6 copy-start.4
Sparse Core Ops, SparseCore 0:
  27.0 39.9 reduce-scatter.2
  70.5 28.4 all-gather.3
  101.1 124.4 all-gather.5
  227.5 123.1 all-gather.7
  362.7 36.0 reduce-scatter.4
where the time goes:
time: 409 us
  waiting for transfers between devices  344 us (84%)
  matrix products  31.1 us (8%)
  between operations  13.3 us (3%)
  other arithmetic  10 us (2%)
  starting transfers between devices  5.86 us (1%)
  local copies, waits for them, and re-layouts  4.69 us (1%)
    all_gather x1, waiting for transfers between devices, on_device(): lax.all_gather(up_weight, 'sp', axis=0, tiled=True)  127 us
    all_gather x1, waiting for transfers between devices, on_device(): lax.all_gather(down_weight, 'sp', axis=1, tiled=True)  113 us
    reduce_scatter x1, waiting for transfers between devices, on_device(): lax.psum_scatter(jnp.dot(attended, out_weight, preferred_element_type=jnp...  39.3 us
    reduce_scatter x1, waiting for transfers between devices, on_device(): lax.psum_scatter(terms.astype(jnp.bfloat16), 'tp', scatter_dimension=0, t...  36.2 us
    all_gather x1, waiting for transfers between devices, on_device(): whole = lax.all_gather(normed, 'tp', axis=0, tiled=True)  27.1 us
    dot_general x1, matrix products, on_device(): upward = jnp.dot(whole, up_full, preferred_element_type=jnp.float32)  11.9 us
    dot_general x1, matrix products, on_device(): terms = jnp.dot(act, down_full, preferred_element_type=jnp.float32)  11.8 us
  transfers between devices with their start and end apart: 6, of which 5 were waited for; matrix products, arithmetic and copies ran while one was open for 3% of the time, Pallas kernels for 0%

commit v1 on v0

--- a/solution.py
+++ b/solution.py
@@ -1,6 +1,10 @@
+import functools
+
 import jax
 import jax.numpy as jnp
 from jax import lax
+from jax.experimental import pallas as pl
+from jax.experimental.pallas import tpu as pltpu
 from jax.sharding import PartitionSpec as P
 
 HEADS = 12
@@ -70,21 +74,257 @@
     return attended.astype(jnp.bfloat16).reshape(tokens, heads_local * HEAD)
 
 
+MESH = pl.DeviceIdType.MESH
+LANES = 128
+
+
+def norm_rows(stream, gain, bias):
+    mean = jnp.mean(stream, axis=-1, keepdims=True)
+    spread = jnp.mean(jnp.square(stream - mean), axis=-1, keepdims=True)
+    return (stream - mean) * lax.rsqrt(spread + norm_eps) * gain + bias
+
+
+def block_kernel(
+    n, m, up_ref, down_ref, mix_ref, res_ref, gains_ref, biases_ref, out_ref,
+    up_all, down_all, mix_in, normed, act, terms, terms_in, total,
+    ring_send, ring_recv, mix_send, mix_recv, row_send, row_recv, sum_send, sum_recv,
+):
+    me, rank = lax.axis_index("sp"), lax.axis_index("tp")
+    depth, hidden = up_ref.shape
+    half = depth // 2
+    own_rows, width = res_ref.shape
+    step_rows = 32
+
+    odd = lax.rem(me, 2)
+    place = (1 - odd) * lax.div(me, 2) + odd * (n - 1 - lax.div(me, 2))
+
+    def member(at):
+        at = lax.rem(at + n, n)
+        back = lax.div(at, n // 2)
+        return (1 - back) * (2 * at) + back * (2 * (n - 1 - at) + 1)
+
+    right, left = member(place + 1), member(place - 1)
+
+    def peer(k):
+        return lax.rem(rank + k, m)
+
+    barrier = pltpu.get_barrier_semaphore()
+    for there in (left, right):
+        pl.semaphore_signal(barrier, inc=1, device_id=(there, rank), device_id_type=MESH)
+    for k in range(1, m):
+        pl.semaphore_signal(barrier, inc=1, device_id=(me, peer(k)), device_id_type=MESH)
+    pl.semaphore_wait(barrier, m + 1)
+
+    def remote(source, target, send, recv, device):
+        return pltpu.make_async_remote_copy(
+            src_ref=source, dst_ref=target, send_sem=send, recv_sem=recv,
+            device_id=device, device_id_type=MESH,
+        )
+
+    def hop(which, s, d, c):
+        owner = member(place - s) if d == 0 else member(place + s)
+        if which == 0:
+            rows = half // 2
+            off = d * half + c * rows
+            target = up_all.at[pl.ds(pl.multiple_of(owner * depth + off, rows), rows)]
+            source = up_ref.at[pl.ds(off, rows)] if s == 0 else target
+        else:
+            rows = hidden // 2
+            target = down_all.at[2 * owner + d, pl.ds(c * rows, rows)]
+            source = target
+            if s == 0:
+                source = down_ref.at[pl.ds(c * rows, rows), pl.ds(d * half, half)]
+        return remote(
+            source, target, ring_send.at[which, s, d, c], ring_recv.at[which, s, d, c],
+            (right if d == 0 else left, rank),
+        )
+
+    def launch(which):
+        for c in range(2):
+            for d in range(2):
+                hop(which, 0, d, c).start()
+
+    def serve(which, s, c):
+        for d in range(2):
+            hop(which, s, d, c).wait_recv()
+            if s + 1 < n - 1:
+                hop(which, s + 1, d, c).start()
+
+    def serve_up(s):
+        for c in range(2):
+            serve(0, s, c)
+        if s == max(n - 3, 0):
+            launch(1)
+
+    launch(0)
+    mix_copies = [
+        remote(
+            mix_ref.at[pl.ds(pl.multiple_of(peer(k) * own_rows, own_rows), own_rows)],
+            mix_in.at[k - 1], mix_send.at[k - 1], mix_recv.at[k - 1], (me, peer(k)),
+        )
+        for k in range(1, m)
+    ]
+    for copy in mix_copies:
+        copy.start()
+    up_all[pl.ds(pl.multiple_of(me * depth, depth), depth)] = up_ref[...]
+    for d in range(2):
+        down_all[2 * me + d] = down_ref[:, d * half : (d + 1) * half]
+
+    early = (n - 1) // 2
+    for s in range(early):
+        serve_up(s)
+    for copy in mix_copies:
+        copy.wait_recv()
+
+    @pl.loop(0, own_rows // step_rows)
+    def _(i):
+        start = pl.multiple_of(i * step_rows, step_rows)
+        rows = pl.ds(start, step_rows)
+        mine = pl.ds(pl.multiple_of(rank * own_rows + start, step_rows), step_rows)
+        mix = mix_ref[mine].astype(jnp.float32)
+        for k in range(m - 1):
+            mix += mix_in[k, rows].astype(jnp.float32)
+        stream = deep_alpha * res_ref[rows].astype(jnp.float32) + mix
+        normed[mine] = norm_rows(stream, gains_ref[0:1], biases_ref[0:1]).astype(jnp.bfloat16)
+
+    held = pl.ds(pl.multiple_of(rank * own_rows, own_rows), own_rows)
+    row_copies = [
+        remote(
+            normed.at[held], normed.at[held], row_send.at[k - 1], row_recv.at[k - 1], (me, peer(k))
+        )
+        for k in range(1, m)
+    ]
+    for copy in row_copies:
+        copy.start()
+    for s in range(early, n - 1):
+        serve_up(s)
+    for copy in row_copies:
+        copy.wait_recv()
+
+    tile = 256
+    tiles = hidden // tile
+    parts = 4
+
+    def upward(first, last):
+        @pl.loop(first, last)
+        def _(i):
+            columns = pl.ds(pl.multiple_of(i * tile, tile), tile)
+            made = jnp.dot(normed[...], up_all[:, columns], preferred_element_type=jnp.float32)
+            act[:, columns] = jnp.square(jnp.maximum(made, 0.0)).astype(jnp.bfloat16)
+
+    for part in range(parts):
+        upward(part * tiles // parts, (part + 1) * tiles // parts)
+        if part < 2:
+            serve(1, 0, part)
+
+    def owners(j):
+        return member(place - j), member(place + j)
+
+    def share(j, k):
+        return remote(
+            terms.at[j, :, pl.ds(pl.multiple_of(peer(k) * own_rows, own_rows), own_rows)],
+            terms_in.at[k - 1, j], sum_send.at[k - 1, j], sum_recv.at[k - 1, j], (me, peer(k)),
+        )
+
+    def downward(j):
+        for d, owner in enumerate(owners(j)):
+            terms[j, d] = jnp.dot(
+                act[...], down_all[2 * owner + d], preferred_element_type=jnp.float32
+            ).astype(jnp.bfloat16)
+        for k in range(1, m):
+            share(j, k).start()
+
+    def collect(j):
+        for k in range(1, m):
+            share(j, k).wait_recv()
+        for d, owner in enumerate(owners(j)):
+            columns = pl.ds(pl.multiple_of(owner * depth + d * half, half), half)
+            block = terms[j, d, held].astype(jnp.float32)
+            for k in range(m - 1):
+                block += terms_in[k, j, d].astype(jnp.float32)
+            total[:, columns] = deep_alpha * normed[held, columns].astype(jnp.float32) + block
+
+    downward(0)
+    downward(1)
+    for s in range(1, n - 1):
+        for c in range(2):
+            serve(1, s, c)
+        downward(s + 1)
+        collect(s - 1)
+    collect(n - 2)
+    collect(n - 1)
+
+    @pl.loop(0, own_rows // step_rows)
+    def _(i):
+        rows = pl.ds(pl.multiple_of(i * step_rows, step_rows), step_rows)
+        out_ref[rows] = norm_rows(total[rows], gains_ref[1:2], biases_ref[1:2]).astype(jnp.bfloat16)
+
+    for copy in mix_copies + row_copies:
+        copy.wait_send()
+    for j in range(n):
+        for k in range(1, m):
+            share(j, k).wait_send()
+    for which in range(2):
+        for s in range(n - 1):
+            for d in range(2):
+                for c in range(2):
+                    hop(which, s, d, c).wait_send()
+
+
+def fused_block(up_weight, down_weight, mix, residual, gains, biases):
+    n, m = lax.axis_size("sp"), lax.axis_size("tp")
+    depth, hidden = up_weight.shape
+    half = depth // 2
+    tokens, width = mix.shape
+    own_rows = residual.shape[0]
+    bf16, dma = jnp.bfloat16, pltpu.SemaphoreType.DMA
+    return pl.pallas_call(
+        functools.partial(block_kernel, n, m),
+        out_shape=jax.ShapeDtypeStruct(residual.shape, bf16),
+        in_specs=[pl.BlockSpec(memory_space=pltpu.VMEM)] * 6,
+        out_specs=pl.BlockSpec(memory_space=pltpu.VMEM),
+        scratch_shapes=[
+            pltpu.VMEM((width, hidden), bf16),
+            pltpu.VMEM((2 * n, hidden, half), bf16),
+            pltpu.VMEM((m - 1, own_rows, width), bf16),
+            pltpu.VMEM((tokens, width), bf16),
+            pltpu.VMEM((tokens, hidden), bf16),
+            pltpu.VMEM((n, 2, tokens, half), bf16),
+            pltpu.VMEM((m - 1, n, 2, own_rows, half), bf16),
+            pltpu.VMEM((own_rows, width), jnp.float32),
+            dma((2, n - 1, 2, 2)),
+            dma((2, n - 1, 2, 2)),
+            dma((m - 1,)),
+            dma((m - 1,)),
+            dma((m - 1,)),
+            dma((m - 1,)),
+            dma((m - 1, n)),
+            dma((m - 1, n)),
+        ],
+        compiler_params=pltpu.CompilerParams(
+            collective_id=0, has_side_effects=True, vmem_limit_bytes=60 * 1024 * 1024
+        ),
+    )(up_weight, down_weight, mix, residual, gains, biases)
+
+
 def on_device(
     queries, keys, values, residual, sinks, out_weight, up_weight, down_weight, gains, biases
 ):
     tokens = queries.shape[0]
     rank_tp = lax.axis_index("tp")
+    tails = jnp.stack([keys[tokens - WINDOW :], values[tokens - WINDOW :]])
+    before = from_behind(tails, "sp", 1)
+    offset = lax.axis_index("sp") * tokens
+    attended = attend(queries, keys, values, before, sinks, offset, rank_tp)
+    part = jnp.dot(attended, out_weight, preferred_element_type=jnp.float32).astype(jnp.bfloat16)
+    if up_weight.shape[0] % (2 * LANES) == 0 and lax.axis_size("sp") % 2 == 0:
+        return fused_block(up_weight, down_weight, part, residual, gains, biases)
     up_full, down_full = (
         lax.all_gather(up_weight, "sp", axis=0, tiled=True),
         lax.all_gather(down_weight, "sp", axis=1, tiled=True),
     )
-    tails = jnp.stack([keys[tokens - WINDOW :], values[tokens - WINDOW :]])
-    before = from_behind(tails, "sp", 1)
-    offset = lax.axis_index("sp") * tokens
-    attended = attend(queries, keys, values, before, sinks, offset, rank_tp)
     mix = lax.psum_scatter(
-        jnp.dot(attended, out_weight, preferred_element_type=jnp.float32).astype(jnp.bfloat16),
+        part,
         "tp",
         scatter_dimension=0,
         tiled=True,

time: 409 us -> 196 us (0.48)
  waiting for transfers between devices: 344 us -> 0.01 us
  Pallas kernels: 0 us -> 174 us
  matrix products: 31.1 us -> 6.34 us
  between operations: 13.3 us -> 0.15 us
  other arithmetic: 10 us -> 1.69 us
    all_gather x3 -> x0, waiting for transfers between devices: 267 us -> none  [the longest x1 127 us: on_device(): lax.all_gather(up_weight, 'sp', axis=0, tiled=True)]
    pallas_call x0 -> x1, Pallas kernels: none -> 174 us  [fused_block(): pl.pallas_call(functools.partial(block_kernel, n, m), out_shape=jax.Shape...]
    reduce_scatter x2 -> x0, waiting for transfers between devices: 75.6 us -> none  [the longest x1 39.3 us: on_device(): lax.psum_scatter(jnp.dot(attended, out_weight, preferred_element_type=jnp...]
    dot_general x2 -> x0, matrix products: 23.7 us -> none  [the longest x1 11.9 us: on_device(): upward = jnp.dot(whole, up_full, preferred_element_type=jnp.float32)]
  transfers between devices with their start and end apart: 6 -> 1, of which waited for: 5 -> 0; matrix products, arithmetic and copies ran while one was open for 3% -> 1% of each run, Pallas kernels for 0% -> 0%
where the time goes in v1:
time: 196 us; the launch traced here: 195 us
  Pallas kernels  174 us (89%)
  local copies, waits for them, and re-layouts  7.9 us (4%)
  matrix products  6.34 us (3%)
  starting transfers between devices  5.52 us (3%)
    pallas_call x1, Pallas kernels, fused_block(): pl.pallas_call(functools.partial(block_kernel, n, m), out_shape=jax.Shape...  174 us
    ppermute x1, starting transfers between devices, from_behind(): return lax.ppermute(block, axis, route)  5.52 us
  transfers between devices with their start and end apart: 1, of which 0 were waited for; matrix products, arithmetic and copies ran while one was open for 1% of the time, Pallas kernels for 0%

profile of v1, /device:TPU:0, one launch (start us, length us, event | category | flops | bytes accessed | tf_op | source)
XLA Modules:
  0.0 195.2 jit_solution(9207383597530851365)
XLA Ops:
  0.0 0.9 slice_bitcast_fusion.2
  0.9 0.6 pad_maximum_fusion.2
  1.6 5.5 %collective-permute-start = (bf16[2,128,128]{2,1,0:T(8,128)(2,1)}, bf16[2,128,128]{2,1,0:T(8,128)(2,1)}, u32[]{:S(2)}, u32[]{:S(2)}) collective-permute-start(bf16[2,128,128]{2,1,0:T(8,128)(2,1)} %pad_maximum_fusion.2), channel_id=1, source_target_pairs={{0,4},{4,8},{8,12},{12,16},{16,20},{20,24},{24,28},{1,5},{5,9},{9,... | collective-permute-start | bytes 196616 | tf_op jit(solution)/shard_map/ppermute | solution.py:23
  7.2 0.1 add_compare_fusion
  7.3 0.1 broadcast_multiply_fusion
  7.4 0.3 broadcast_and_fusion
  7.6 2.0 %reshape.182 = bf16[6,128,3,128]{3,2,1,0:T(4,128)(2,1)S(1)} reshape(bf16[768,384]{1,0:T(8,128)(2,1)} %param.10) | data formatting | bytes 1179648 | tf_op jit(solution)/shard_map/reshape.20
  9.7 0.0 copy-done.2
  9.7 0.2 copy.14
  9.8 0.0 collective-permute-done
  9.8 0.8 slice_bitcast_fusion.1
  10.7 0.0 copy-start.4
  10.7 0.7 fusion.17
  11.3 0.1 broadcast_maximum_fusion
  11.4 1.3 copy-done.1
  12.7 0.4 fusion.1
  13.1 0.1 exponential_add_fusion
  13.2 0.2 copy.13
  13.4 2.2 %fusion.2 = bf16[6,128,1,3,128]{1,4,3,0,2:T(8,128)(2,1)S(1)} fusion(f32[6,1,3,128,256]{3,4,2,0,1:T(8,128)} %copy-done.1, f32[6,3,128]{2,1,0:T(4,128)S(1)} %exponential_add_fusion, f32[6,3,128]{2,1,0:T(4,128)S(1)} %broadcast_maximum_fusion, bf16[6,128,1,128]{1,3,0,2:T(8,128)(2,1)S(1)} %copy.14, bf16[6,128,1,128]{1,3,0,2:T(8,128)(2,1)S(1)} %copy.13), kind=kOutput, calls=%fused_computation.7 | convolution fusion | flops 153845760 | bytes 3360768 | tf_op jit(solution)/shard_map/nkgqs,nskd->nqkgd/dot_general | solution.py:73
  15.6 0.4 copy.18
  16.0 0.0 copy-done
  16.0 3.5 %convolution_convert_fusion.mix_ref = bf16[768,2048]{1,0:T(8,128)(2,1)} fusion(bf16[384,2048]{1,0:T(8,128)(2,1)S(1)} %copy-done, bf16[48,8,6,128]{3,2,1,0:T(8,128)(2,1)S(1)} %bitcast.49), kind=kOutput, calls=%fused_computation | convolution fusion | flops 1209532416 | bytes 5308416 | tf_op jit(solution)/shard_map/dot_general | solution.py:319
  19.5 173.6 %shard_map.100 = bf16[192,2048]{1,0:T(8,128)(2,1)} custom-call(bf16[256,2048]{1,0:T(8,128)(2,1)} %up_ref.1, bf16[2048,256]{1,0:T(8,128)(2,1)} %down_ref.1, bf16[768,2048]{1,0:T(8,128)(2,1)} %convolution_convert_fusion.mix_ref, bf16[192,2048]{1,0:T(8,128)(2,1)} %res_ref.1, f32[2,2048]{1,0:T(2,128)} %gains_ref.1, f32[2,2048]{1,0:T(2,128)} %biases_ref.1), custom_call_target="tpu_custom_call" | custom-call | tf_op jit(solution)/shard_map/pallas_call | solution.py:281
  193.1 2.1 %copy.34 = bf16[192,2048]{1,0:T(8,128)(2,1)} copy(bf16[192,2048]{1,0:T(8,128)(2,1)} %shard_map.100) | data formatting | bytes 1572864
  (13 shorter events, 0.1 us)
Async XLA Ops:
  0.0 16.0 %copy-start = (bf16[384,2048]{1,0:T(8,128)(2,1)S(1)}, bf16[384,2048]{1,0:T(8,128)(2,1)}, u32[]{:S(2)}) copy-start(bf16[384,2048]{1,0:T(8,128)(2,1)} %param.15) | copy-start | bytes 4718596
  0.0 10.6 %copy-start.3 = (bf16[768,128]{1,0:T(8,128)(2,1)S(1)}, bf16[768,128]{1,0:T(8,128)(2,1)}, u32[]{:S(2)}) copy-start(bf16[768,128]{1,0:T(8,128)(2,1)} %param.11) | copy-start | bytes 589828
  0.0 9.7 %copy-start.2 = (bf16[768,128]{1,0:T(8,128)(2,1)S(1)}, bf16[768,128]{1,0:T(8,128)(2,1)}, u32[]{:S(2)}) copy-start(bf16[768,128]{1,0:T(8,128)(2,1)} %param.12) | copy-start | bytes 589828
  1.6 8.3 %collective-permute-start = (bf16[2,128,128]{2,1,0:T(8,128)(2,1)}, bf16[2,128,128]{2,1,0:T(8,128)(2,1)}, u32[]{:S(2)}, u32[]{:S(2)}) collective-permute-start(bf16[2,128,128]{2,1,0:T(8,128)(2,1)} %pad_maximum_fusion.2), channel_id=1, source_target_pairs={{0,4},{4,8},{8,12},{12,16},{16,20},{20,24},{24,28},{1,5},{5,9},{9,... | collective-permute-start | bytes 196616 | tf_op jit(solution)/shard_map/ppermute | solution.py:23
  10.7 0.7 copy-start.4
  11.3 1.4 copy-start.1

commit v2 on v1

--- a/solution.py
+++ b/solution.py
@@ -85,9 +85,9 @@
 
 
 def block_kernel(
-    n, m, up_ref, down_ref, mix_ref, res_ref, gains_ref, biases_ref, out_ref,
-    up_all, down_all, mix_in, normed, act, terms, terms_in, total,
-    ring_send, ring_recv, mix_send, mix_recv, row_send, row_recv, sum_send, sum_recv,
+    n, m, q_ref, k_ref, v_ref, sinks_ref, slopes_ref, proj_ref, up_ref, down_ref, res_ref,
+    gains_ref, biases_ref, out_ref, key_ext, val_ext, attended, mix_ref, up_all, down_all, mix_in, normed, act, terms, terms_in, total,
+    tail_send, tail_recv, ring_send, ring_recv, mix_send, mix_recv, row_send, row_recv, sum_send, sum_recv,
 ):
     me, rank = lax.axis_index("sp"), lax.axis_index("tp")
     depth, hidden = up_ref.shape
@@ -109,11 +109,12 @@
         return lax.rem(rank + k, m)
 
     barrier = pltpu.get_barrier_semaphore()
-    for there in (left, right):
+    after, ahead = lax.rem(me + 1, n), lax.rem(me + n - 1, n)
+    for there in (left, right, after, ahead):
         pl.semaphore_signal(barrier, inc=1, device_id=(there, rank), device_id_type=MESH)
     for k in range(1, m):
         pl.semaphore_signal(barrier, inc=1, device_id=(me, peer(k)), device_id_type=MESH)
-    pl.semaphore_wait(barrier, m + 1)
+    pl.semaphore_wait(barrier, m + 3)
 
     def remote(source, target, send, recv, device):
         return pltpu.make_async_remote_copy(
@@ -156,7 +157,69 @@
         if s == max(n - 3, 0):
             launch(1)
 
+    tokens = q_ref.shape[0]
+    tails = [
+        remote(
+            ref.at[pl.ds(tokens - WINDOW, WINDOW)], ext.at[pl.ds(0, WINDOW)],
+            tail_send.at[i], tail_recv.at[i], (after, rank),
+        )
+        for i, (ref, ext) in enumerate(((k_ref, key_ext), (v_ref, val_ext)))
+    ]
+    for copy in tails:
+        copy.start()
     launch(0)
+    key_ext[WINDOW:] = k_ref[...]
+    val_ext[WINDOW:] = v_ref[...]
+    up_all[pl.ds(pl.multiple_of(me * depth, depth), depth)] = up_ref[...]
+    for d in range(2):
+        down_all[2 * me + d] = down_ref[:, d * half : (d + 1) * half]
+    for copy in tails:
+        copy.wait_recv()
+
+    blocks = tokens // WINDOW
+    heads_local = q_ref.shape[1] // HEAD
+    group = heads_local // (k_ref.shape[1] // HEAD)
+
+    def windows(first, last):
+        @pl.loop(first, last)
+        def _(i):
+            start = pl.multiple_of(i * WINDOW, WINDOW)
+            rows, span = pl.ds(start, WINDOW), pl.ds(start, 2 * WINDOW)
+            q_index = lax.broadcasted_iota(jnp.int32, (WINDOW, 2 * WINDOW), 0)
+            k_index = lax.broadcasted_iota(jnp.int32, (WINDOW, 2 * WINDOW), 1)
+            dist = q_index + WINDOW - k_index
+            key_pos = me * tokens + start - WINDOW + k_index
+            valid = (dist >= 0) & (dist < WINDOW) & (key_pos >= 0)
+            far = dist.astype(jnp.float32)
+            for h in range(heads_local):
+                columns = slice(h * HEAD, (h + 1) * HEAD)
+                shared = slice(h // group * HEAD, (h // group + 1) * HEAD)
+                logits = lax.dot_general(
+                    q_ref[rows, columns], key_ext[span, shared], (((1,), (1,)), ((), ())),
+                    preferred_element_type=jnp.float32,
+                ) * HEAD ** (-0.5)
+                logits = jnp.where(valid, logits - slopes_ref[h] * far, neg_big)
+                sink = sinks_ref[h]
+                top = jnp.maximum(jnp.max(logits, axis=-1, keepdims=True), sink)
+                probs = jnp.exp(logits - top)
+                denom = jnp.sum(probs, axis=-1, keepdims=True) + jnp.exp(sink - top)
+                weight = (probs / denom).astype(jnp.bfloat16)
+                attended[rows, columns] = jnp.dot(
+                    weight, val_ext[span, shared], preferred_element_type=jnp.float32
+                ).astype(jnp.bfloat16)
+
+    windows(0, blocks // 2)
+    serve(0, 0, 0)
+    windows(blocks // 2, blocks)
+    serve(0, 0, 1)
+
+    @pl.loop(0, width // (2 * LANES))
+    def _(i):
+        columns = pl.ds(pl.multiple_of(i * 2 * LANES, 2 * LANES), 2 * LANES)
+        mix_ref[:, columns] = jnp.dot(
+            attended[...], proj_ref[:, columns], preferred_element_type=jnp.float32
+        ).astype(jnp.bfloat16)
+
     mix_copies = [
         remote(
             mix_ref.at[pl.ds(pl.multiple_of(peer(k) * own_rows, own_rows), own_rows)],
@@ -166,12 +229,9 @@
     ]
     for copy in mix_copies:
         copy.start()
-    up_all[pl.ds(pl.multiple_of(me * depth, depth), depth)] = up_ref[...]
-    for d in range(2):
-        down_all[2 * me + d] = down_ref[:, d * half : (d + 1) * half]
-
-    early = (n - 1) // 2
-    for s in range(early):
+
+    early = n // 2
+    for s in range(1, early):
         serve_up(s)
     for copy in mix_copies:
         copy.wait_recv()
@@ -259,7 +319,7 @@
         rows = pl.ds(pl.multiple_of(i * step_rows, step_rows), step_rows)
         out_ref[rows] = norm_rows(total[rows], gains_ref[1:2], biases_ref[1:2]).astype(jnp.bfloat16)
 
-    for copy in mix_copies + row_copies:
+    for copy in tails + mix_copies + row_copies:
         copy.wait_send()
     for j in range(n):
         for k in range(1, m):
@@ -271,19 +331,26 @@
                     hop(which, s, d, c).wait_send()
 
 
-def fused_block(up_weight, down_weight, mix, residual, gains, biases):
+def fused_block(
+    queries, keys, values, sinks, slopes, out_weight, up_weight, down_weight, residual, gains, biases
+):
     n, m = lax.axis_size("sp"), lax.axis_size("tp")
     depth, hidden = up_weight.shape
     half = depth // 2
-    tokens, width = mix.shape
-    own_rows = residual.shape[0]
+    tokens = queries.shape[0]
+    own_rows, width = residual.shape
+    vmem, smem = pl.BlockSpec(memory_space=pltpu.VMEM), pl.BlockSpec(memory_space=pltpu.SMEM)
     bf16, dma = jnp.bfloat16, pltpu.SemaphoreType.DMA
     return pl.pallas_call(
         functools.partial(block_kernel, n, m),
         out_shape=jax.ShapeDtypeStruct(residual.shape, bf16),
-        in_specs=[pl.BlockSpec(memory_space=pltpu.VMEM)] * 6,
+        in_specs=[vmem] * 3 + [smem] * 2 + [vmem] * 6,
         out_specs=pl.BlockSpec(memory_space=pltpu.VMEM),
         scratch_shapes=[
+            pltpu.VMEM((tokens + WINDOW, keys.shape[1]), bf16),
+            pltpu.VMEM((tokens + WINDOW, keys.shape[1]), bf16),
+            pltpu.VMEM(queries.shape, bf16),
+            pltpu.VMEM((tokens, width), bf16),
             pltpu.VMEM((width, hidden), bf16),
             pltpu.VMEM((2 * n, hidden, half), bf16),
             pltpu.VMEM((m - 1, own_rows, width), bf16),
@@ -292,6 +359,8 @@
             pltpu.VMEM((n, 2, tokens, half), bf16),
             pltpu.VMEM((m - 1, n, 2, own_rows, half), bf16),
             pltpu.VMEM((own_rows, width), jnp.float32),
+            dma((2,)),
+            dma((2,)),
             dma((2, n - 1, 2, 2)),
             dma((2, n - 1, 2, 2)),
             dma((m - 1,)),
@@ -304,7 +373,10 @@
         compiler_params=pltpu.CompilerParams(
             collective_id=0, has_side_effects=True, vmem_limit_bytes=60 * 1024 * 1024
         ),
-    )(up_weight, down_weight, mix, residual, gains, biases)
+    )(
+        queries, keys, values, sinks, slopes, out_weight, up_weight, down_weight, residual, gains,
+        biases,
+    )
 
 
 def on_device(
@@ -312,13 +384,19 @@
 ):
     tokens = queries.shape[0]
     rank_tp = lax.axis_index("tp")
+    if up_weight.shape[0] % (2 * LANES) == 0 and lax.axis_size("sp") % 2 == 0:
+        heads_local = sinks.shape[0]
+        heads = (jnp.arange(heads_local, dtype=jnp.int32) + rank_tp * heads_local).astype(jnp.float32)
+        slopes = jnp.exp2(-8.0 * (heads + 1.0) / HEADS)
+        return fused_block(
+            queries, keys, values, sinks, slopes, out_weight, up_weight, down_weight, residual,
+            gains, biases,
+        )
     tails = jnp.stack([keys[tokens - WINDOW :], values[tokens - WINDOW :]])
     before = from_behind(tails, "sp", 1)
     offset = lax.axis_index("sp") * tokens
     attended = attend(queries, keys, values, before, sinks, offset, rank_tp)
     part = jnp.dot(attended, out_weight, preferred_element_type=jnp.float32).astype(jnp.bfloat16)
-    if up_weight.shape[0] % (2 * LANES) == 0 and lax.axis_size("sp") % 2 == 0:
-        return fused_block(up_weight, down_weight, part, residual, gains, biases)
     up_full, down_full = (
         lax.all_gather(up_weight, "sp", axis=0, tiled=True),
         lax.all_gather(down_weight, "sp", axis=1, tiled=True),

time: 196 us -> 181 us (0.923)
  matrix products: 6.34 us -> 0 us
  local copies, waits for them, and re-layouts: 7.9 us -> 2.09 us
  starting transfers between devices: 5.52 us -> 0 us
  Pallas kernels: 174 us -> 176 us
    dot_general x3 -> x0, matrix products: 6.34 us -> none  [the longest x1 3.49 us: on_device(): jnp.dot(attended, out_weight, preferred_element_type=jnp.float32)]
    ppermute x1 -> x0, starting transfers between devices: 5.52 us -> none  [from_behind(): return lax.ppermute(block, axis, route)]
    another operation x2 -> x0, local copies, waits for them, and re-layouts: 2.92 us -> none
    pallas_call x1, Pallas kernels: 174 us -> 176 us  [fused_block(): pl.pallas_call(functools.partial(block_kernel, n, m), out_shape=jax.Shape...]
  transfers between devices with their start and end apart: 1 -> 0, of which waited for: 0 -> 0; matrix products, arithmetic and copies ran while one was open for 1% -> 0% of each run, Pallas kernels for 0% -> 0%
where the time goes in v2:
time: 181 us; the launch traced here: 179 us
  Pallas kernels  176 us (97%)
  local copies, waits for them, and re-layouts  2.09 us (1%)
    pallas_call x1, Pallas kernels, fused_block(): pl.pallas_call(functools.partial(block_kernel, n, m), out_shape=jax.Shape...  176 us

profile of v2, /device:TPU:0, one launch (start us, length us, event | category | flops | bytes accessed | tf_op | source)
XLA Modules:
  0.0 178.9 jit_solution(12671939969960642474)
XLA Ops:
  0.0 0.5 multiply_exponential_fusion.slopes_ref
  0.5 176.3 %shard_map.100 = bf16[192,2048]{1,0:T(8,128)(2,1)} custom-call(bf16[768,384]{1,0:T(8,128)(2,1)} %q_ref.1, bf16[768,128]{1,0:T(8,128)(2,1)} %k_ref.1, bf16[768,128]{1,0:T(8,128)(2,1)} %v_ref.1, f32[3]{0:T(128)} %sinks_ref.1, f32[3]{0:T(128)} %multiply_exponential_fusion.slopes_ref, bf16[384,2048]{1,0:T(8,128)(2,1)} %proj_ref.1, bf16[256,2048]{1,0:T(8,128)(2,1)} %up_ref.1, ...), custom_call_target="tpu_custom_call" | custom-call | tf_op jit(solution)/shard_map/pallas_call | solution.py:344
  176.8 2.1 %copy.12 = bf16[192,2048]{1,0:T(8,128)(2,1)} copy(bf16[192,2048]{1,0:T(8,128)(2,1)} %shard_map.100) | data formatting | bytes 1572864
